TPU v7x, 512 devices: a whole 4x8x8 slice. The times are simulated.
512 devices in a mesh: sp: 64 (over z, y), tp: 8 (over x, core).
Axes of the slice: x: 4, y: 8, z: 8, core: 2. Of those that a mesh axis runs over, the one named last changes fastest.
Arguments:
- latent: bfloat16 [16384, 2048], P('sp'), may hold values from -6 to 6
- context: bfloat16 [512, 2048], P('sp'), may hold values from -6 to 6
- cond: bfloat16 [2048], P('sp'), may hold values from -6 to 6
- cond_ctx: bfloat16 [2048], P('sp'), may hold values from -6 to 6
- shift_weight: bfloat16 [2048, 2048], P('sp', 'tp'), may hold values from -0.125 to 0.125
- scale_weight: bfloat16 [2048, 2048], P('sp', 'tp'), may hold values from -0.125 to 0.125
- gate_weight: bfloat16 [2048, 2048], P('sp', 'tp'), may hold values from -0.25 to 0.25
- norm_gain: bfloat16 [2048], replicated, may hold values from 0.099609375 to 1.8984375
- query_weight: bfloat16 [2048, 1024], P(None, 'tp'), may hold values from -0.125 to 0.125
- key_weight: bfloat16 [2048, 1024], P(None, 'tp'), may hold values from -0.125 to 0.125
- value_weight: bfloat16 [2048, 1024], P(None, 'tp'), may hold values from -0.125 to 0.125
- query_gain: bfloat16 [64], replicated, may hold values from 0.099609375 to 1.8984375
- key_gain: bfloat16 [64], replicated, may hold values from 0.099609375 to 1.8984375
- offset_bias: float32 [16, 15, 31], P('tp'), may hold values from -0.5 to 251
- out_weight: bfloat16 [1024, 2048], P(None, 'tp'), may hold values from -1.5 to 1.5
Outputs:
- updated: bfloat16 [16384, 2048], P('sp', 'tp')
All inputs are finite; a program needn't handle non-finite values.
Results may differ from a plain program's by a relative error of at most 0.0077.
Values may be sent and summed in bfloat16 or wider, within the bound.
A program may use at most 64 MiB of HBM per device.

v0:
```python
import jax
import jax.numpy as jnp
import numpy as np
from jax import lax
from jax.sharding import Mesh
from jax.sharding import PartitionSpec as P

HEAD_DIM = 64
WIN_ROWS = 8
WIN_COLS = 16
GRID_W = 64
SP = ("sp_0", "sp_1")
EPS = 1e-06


def one_axis_at_a_time(x, axes):
    for axis in axes:
        x = lax.psum(x, axis)
    return x


def in_order(pieces, dim):
    dims = list(pieces.shape[1:])
    dims[dim] *= pieces.shape[0]
    return jnp.moveaxis(pieces, 0, dim).reshape(dims)


def sent_to_all(x, axis):
    copies = jnp.broadcast_to(x, (lax.axis_size(axis), *x.shape))
    return lax.all_to_all(copies, axis, split_axis=0, concat_axis=0, tiled=True)


def collect(x, axis, dim):
    return in_order(sent_to_all(x, axis), dim)


def side_by_side(arrays, axis, dim, along):
    widths = [a.shape[along] for a in arrays]
    both = jnp.concatenate(arrays, axis=along)
    result = collect(both, axis, dim)
    return tuple(jnp.split(result, [sum(widths[:k]) for k in range(1, len(widths))], axis=along))


def padded_2(block, sides, width):
    for axis, dim in sides:
        count = lax.axis_size(axis)
        forward = [(i, i + 1) for i in range(count - 1)]
        backward = [(target, source) for source, target in forward]
        low = lax.ppermute(
            lax.slice_in_dim(block, block.shape[dim] - width, None, axis=dim), axis, forward
        )
        high = lax.ppermute(lax.slice_in_dim(block, 0, width, axis=dim), axis, backward)
        block = jnp.concatenate([low, block, high], axis=dim)
    return block


def modulate(rows, norm_gain, scale, shift):
    values = rows.astype(jnp.float32)
    normed = values * lax.rsqrt(jnp.mean(values * values, axis=-1, keepdims=True) + EPS)
    return (normed * norm_gain.astype(jnp.float32) * (1.0 + scale) + shift).astype(jnp.bfloat16)


def project_heads(hidden, weight, gain):
    raw = jnp.dot(hidden, weight, preferred_element_type=jnp.float32)
    split = raw.reshape(hidden.shape[0], -1, HEAD_DIM)
    if gain is None:
        return split.astype(jnp.bfloat16)
    normed = split * lax.rsqrt(jnp.mean(split * split, axis=-1, keepdims=True) + EPS)
    return (normed * gain.astype(jnp.float32)).astype(jnp.bfloat16)


def body(
    latent,
    context,
    cond,
    cond_ctx,
    shift_weight,
    scale_weight,
    gate_weight,
    norm_gain,
    query_weight,
    key_weight,
    value_weight,
    query_gain,
    key_gain,
    offset_bias,
    out_weight,
):
    col_width = shift_weight.shape[1]
    tp_offset = lax.axis_index("tp") * col_width
    act = jax.nn.silu(cond.astype(jnp.float32)).astype(jnp.bfloat16)
    act_ctx = jax.nn.silu(cond_ctx.astype(jnp.float32)).astype(jnp.bfloat16)
    acts = jnp.stack([act, act_ctx])
    terms = jnp.concatenate(
        [
            jnp.dot(acts, shift_weight, preferred_element_type=jnp.float32),
            jnp.dot(acts, scale_weight, preferred_element_type=jnp.float32),
            jnp.dot(acts[:1], gate_weight, preferred_element_type=jnp.float32),
        ],
        axis=0,
    )
    summed = one_axis_at_a_time(terms, SP)
    full = collect(summed, "tp", 1)
    shift, shift_ctx, scale, scale_ctx, gate = (full[0], full[1], full[2], full[3], full[4])
    heads_dev = offset_bias.shape[0]
    lane = heads_dev * HEAD_DIM
    hidden_ctx = modulate(context, norm_gain, scale_ctx, shift_ctx)
    own_keys = project_heads(hidden_ctx, key_weight, key_gain).reshape(context.shape[0], lane)
    own_values = project_heads(hidden_ctx, value_weight, None).reshape(context.shape[0], lane)
    ctx_keys, ctx_values = side_by_side((own_keys, own_values), SP, 0, 1)
    ctx_keys = ctx_keys.reshape(-1, heads_dev, HEAD_DIM)
    ctx_values = ctx_values.reshape(-1, heads_dev, HEAD_DIM)
    hidden = modulate(latent, norm_gain, scale, shift)
    queries = project_heads(hidden, query_weight, query_gain)
    keys = project_heads(hidden, key_weight, key_gain)
    values = project_heads(hidden, value_weight, None)
    rows_dev = latent.shape[0] // GRID_W
    reach = WIN_ROWS // 2
    grid_kv = jnp.stack(
        [keys.reshape(rows_dev, GRID_W, lane), values.reshape(rows_dev, GRID_W, lane)], axis=1
    )
    padded = padded_2(grid_kv, ((SP, 0),), reach)
    total_rows = rows_dev * lax.axis_size(SP)
    base = lax.axis_index(SP) * rows_dev
    local_rows = base + jnp.arange(rows_dev, dtype=jnp.int32)
    first = jnp.clip(local_rows - reach, 0, total_rows - WIN_ROWS)
    window_rows = jnp.arange(WIN_ROWS, dtype=jnp.int32)
    band_index = (first - base + reach)[:, None] + window_rows[None, :]
    band = jnp.take(padded, band_index, axis=0)
    n_blocks = GRID_W // WIN_COLS
    span = 2 * WIN_COLS
    starts = [
        min(max(block * WIN_COLS - WIN_COLS // 2, 0), GRID_W - span) for block in range(n_blocks)
    ]
    blocked = jnp.stack([band[:, :, :, begin : begin + span] for begin in starts], axis=3)
    blocked = blocked.reshape(rows_dev, WIN_ROWS, 2, n_blocks, span, heads_dev, HEAD_DIM)
    key_blocks = blocked[:, :, 0]
    value_blocks = blocked[:, :, 1]
    query_col = np.arange(n_blocks)[:, None, None] * WIN_COLS + np.arange(WIN_COLS)[None, :, None]
    key_col = np.array(starts)[:, None, None] + np.arange(span)[None, None, :]
    window_first = np.clip(query_col - WIN_COLS // 2, 0, GRID_W - WIN_COLS)
    inside = (key_col >= window_first) & (key_col < window_first + WIN_COLS)
    col_offset = np.clip(key_col - query_col + WIN_COLS - 1, 0, 2 * WIN_COLS - 2)
    col_onehot = (col_offset[..., None] == np.arange(2 * WIN_COLS - 1)).astype(np.float32)
    row_offset = first[:, None] + window_rows[None, :] - local_rows[:, None] + WIN_ROWS - 1
    row_onehot = (row_offset[..., None] == jnp.arange(2 * WIN_ROWS - 1, dtype=jnp.int32)).astype(
        jnp.float32
    )
    by_col = jnp.einsum(
        "hxc,bqkc->hxbqk", offset_bias, jnp.asarray(col_onehot), precision=lax.Precision.HIGHEST
    )
    bias = jnp.einsum("rjx,hxbqk->rhbqjk", row_onehot, by_col, precision=lax.Precision.HIGHEST)
    factor = HEAD_DIM ** (-0.5)
    grid_q = queries.reshape(rows_dev, n_blocks, WIN_COLS, heads_dev, HEAD_DIM)
    local_scores = (
        jnp.einsum("rbqhd,rjbkhd->rhbqjk", grid_q, key_blocks, preferred_element_type=jnp.float32)
        * factor
    )
    local_scores = jnp.where(jnp.asarray(inside)[:, :, None, :], local_scores + bias, -jnp.inf)
    band_len = WIN_ROWS * span
    local_scores = local_scores.reshape(rows_dev, heads_dev, n_blocks, WIN_COLS, band_len)
    ctx_scores = (
        jnp.einsum("rbqhd,chd->rhbqc", grid_q, ctx_keys, preferred_element_type=jnp.float32)
        * factor
    )
    scores = jnp.concatenate([local_scores, ctx_scores], axis=-1)
    top = jnp.max(scores, axis=-1, keepdims=True)
    expd = jnp.exp(scores - top)
    weights = (expd / jnp.sum(expd, axis=-1, keepdims=True)).astype(jnp.bfloat16)
    local_w = weights[..., :band_len].reshape(
        rows_dev, heads_dev, n_blocks, WIN_COLS, WIN_ROWS, span
    )
    mixed = jnp.einsum(
        "rhbqjk,rjbkhd->rbqhd", local_w, value_blocks, preferred_element_type=jnp.float32
    )
    mixed = mixed + jnp.einsum(
        "rhbqc,chd->rbqhd", weights[..., band_len:], ctx_values, preferred_element_type=jnp.float32
    )
    mixed = mixed.astype(jnp.bfloat16).reshape(latent.shape[0], lane)
    projected = jnp.dot(collect(mixed, "tp", 1), out_weight, preferred_element_type=jnp.float32)
    own_cols = lax.dynamic_slice_in_dim(latent, tp_offset, col_width, 1).astype(jnp.float32)
    gate_cols = lax.dynamic_slice_in_dim(gate, tp_offset, col_width, 0)
    return (own_cols + gate_cols[None, :] * projected).astype(jnp.bfloat16)


def solution(mesh):
    split = Mesh(mesh.devices.reshape(8, 8, mesh.shape["tp"]), ("sp_0", "sp_1", "tp"))
    placed = (
        P(SP, None),
        P(SP, None),
        P(SP),
        P(SP),
        P(SP, "tp"),
        P(SP, "tp"),
        P(SP, "tp"),
        P(),
        P(None, "tp"),
        P(None, "tp"),
        P(None, "tp"),
        P(),
        P(),
        P("tp", None, None),
        P(None, "tp"),
    )
    return jax.shard_map(body, mesh=split, in_specs=placed, out_specs=P(SP, "tp"), check_vma=False)
```

profile of v0, /device:TPU:1, one launch (start us, length us, event | category | flops | bytes accessed | tf_op | source)
XLA Modules:
  0.0 121.4 jit_solution(677514866326986524)
XLA Ops:
  0.0 0.8 convert_bitcast_fusion
  0.8 0.8 fusion.42
  1.7 0.8 fusion.41
  2.5 0.9 fusion.38
  3.4 20.5 %psum.14 = f32[5,256]{1,0:T(8,128)S(1)} all-reduce(f32[5,256]{1,0:T(8,128)S(1)} %pad_maximum_fusion.2), channel_id=1, replica_groups=mesh['sp_0'=8,'sp_1'=8,'tp'=8] {'sp_0'}, use_global_device_ids=true, to_apply=%region_0.1 | all-reduce | flops 1280 | bytes 10240 | tf_op jit(solution)/shard_map/psum | solution.py:18
  23.9 14.1 %psum.15 = f32[5,256]{1,0:T(8,128)S(1)} all-reduce(f32[5,256]{1,0:T(8,128)S(1)} %psum.14), channel_id=1, replica_groups=mesh['sp_0'=8,'sp_1'=8,'tp'=8] {'sp_1'}, use_global_device_ids=true, to_apply=%region_1.2 | all-reduce | flops 1280 | bytes 10240 | tf_op jit(solution)/shard_map/psum | solution.py:18
  38.0 0.6 broadcast_in_dim.24
  38.6 12.5 %all-to-all-start = ((f32[8,5,256]{2,1,0:T(8,128)}), f32[8,5,256]{2,1,0:T(8,128)S(1)}, u32[]{:S(2)}, u32[]{:S(2)}) async-start(f32[8,5,256]{2,1,0:T(8,128)} %broadcast_in_dim.24), calls=%async_computation | async-start | bytes 131072 | tf_op jit(solution)/shard_map/all_to_all | solution.py:30
  51.3 1.5 %fusion = f32[256]{0:T(256)S(1)} fusion(bf16[256,2048]{1,0:T(8,128)(2,1)} %param.17), kind=kLoop, calls=%fused_computation.3 | loop fusion | flops 1572608 | bytes 1049600 | tf_op jit(solution)/shard_map/reduce_sum | solution.py:59
  52.9 0.9 fusion.25
  53.9 5.6 %convolution_bitcast_fusion = f32[2,15,4,16,32,1]{4,1,5,3,2,0:T(8,128)S(1)} fusion(f32[4,16,32,31,1]{3,2,1,0,4:T(8,128)S(1)} %copy-done.5, f32[2,15,31,1,1]{2,0,1,4,3:T(2,128)} %bitcast.131), kind=kOutput, calls=%fused_computation.20 | convolution fusion | flops 22855680 | bytes 503432 | tf_op jit(solution)/shard_map/hxc,bqkc->hxbqk/dot_general | solution.py:149
  59.5 2.3 %fusion.32 = f32[2,4,16,32,4,8]{3,5,4,2,1,0:T(8,128)} fusion(f32[2,15,4,16,32,1]{4,1,5,3,2,0:T(8,128)S(1)} %convolution_bitcast_fusion, s32[4,8]{1,0:T(4,128)S(1)} %subtract_add_fusion), kind=kOutput, calls=%fused_computation.59 | convolution fusion | flops 23593440 | bytes 770176 | tf_op jit(solution)/shard_map/rjx,hxbqk->rhbqjk/dot_general | solution.py:152
  62.0 0.5 fusion.4
  62.5 0.4 fusion.49
  63.2 0.3 mul.200
  63.8 0.4 convolution_convert_fusion
  64.2 1.8 %collective-permute-start = (bf16[4,2,64,128]{3,2,0,1:T(8,128)(2,1)S(1)}, bf16[4,2,64,128]{3,2,0,1:T(8,128)(2,1)S(1)}, u32[]{:S(2)}, u32[]{:S(2)}) collective-permute-start(bf16[4,2,64,128]{3,2,0,1:T(8,128)(2,1)S(1)} %pad_maximum_fusion.1), channel_id=1, source_target_pairs={{0,8},{8,16},{16,24},{24,32},{32,40},{40,48},{48,56},{56,64},{64,7... | collective-permute-start | bytes 393224 | tf_op jit(solution)/shard_map/ppermute | solution.py:49
  66.0 1.3 %collective-permute-start.1 = (bf16[4,2,64,128]{3,2,0,1:T(8,128)(2,1)S(1)}, bf16[4,2,64,128]{3,2,0,1:T(8,128)(2,1)S(1)}, u32[]{:S(2)}, u32[]{:S(2)}) collective-permute-start(bf16[4,2,64,128]{3,2,0,1:T(8,128)(2,1)S(1)} %pad_maximum_fusion.1), channel_id=1, source_target_pairs={{8,0},{16,8},{24,16},{32,24},{40,32},{48,40},{56,48},{64,56},{72,6... | collective-permute-start | bytes 393224 | tf_op jit(solution)/shard_map/ppermute | solution.py:52
  67.3 0.2 fusion.50
  67.6 0.2 convolution_convert_fusion.1
  67.8 0.5 bitcast_reduce_fusion
  68.8 0.2 reshape.275
  69.1 0.7 broadcast_in_dim.29
  69.8 9.8 %all-to-all-start.1 = ((bf16[64,8,256]{2,1,0:T(8,128)(2,1)}), bf16[64,8,256]{2,1,0:T(8,128)(2,1)}, u32[]{:S(2)}, u32[]{:S(2)}) async-start(bf16[64,8,256]{2,1,0:T(8,128)(2,1)} %broadcast_in_dim.29), calls=%async_computation.1 | async-start | bytes 524288 | tf_op jit(solution)/shard_map/all_to_all | solution.py:30
  79.7 0.7 gather_fusion
  80.6 1.4 %fusion.46 = (bf16[4,8,2,32,128]{4,3,2,1,0:T(8,128)(2,1)S(1)}, bf16[4,8,2,32,128]{4,3,2,1,0:T(8,128)(2,1)}, bf16[4,8,2,32,128]{4,3,2,1,0:T(8,128)(2,1)S(1)}, bf16[4,8,2,32,128]{4,3,2,1,0:T(8,128)(2,1)S(1)}) fusion(bf16[4,8,2,64,128]{4,3,2,1,0:T(8,128)(2,1)S(1)} %broadcast_select_fusion), kind=kLoop, calls=%fused_computation.92 | loop fusion | bytes 4194304 | tf_op jit(solution)/shard_map/slice | solution.py:135
  82.0 0.4 stack.31
  82.4 1.2 copy_dynamic-update-slice_fusion.3
  83.7 0.4 stack.32
  84.1 2.5 %stack.33 = bf16[4,8,2,1,32,2,64]{6,5,4,2,1,0,3:T(2,128)(2,1)S(1)} reshape(bf16[4,8,2,32,128]{4,3,2,1,0:T(8,128)(2,1)} %get-tuple-element.6) | data formatting | bytes 1048576 | tf_op jit(solution)/shard_map/stack | solution.py:135
  86.5 1.4 %stack.34 = bf16[4,8,2,1,32,2,64]{6,5,4,2,1,0,3:T(2,128)(2,1)} reshape(bf16[4,8,2,32,128]{4,3,2,1,0:T(8,128)(2,1)S(1)} %get-tuple-element.5) | data formatting | bytes 1048576 | tf_op jit(solution)/shard_map/stack | solution.py:135
  87.9 1.2 copy_dynamic-update-slice_fusion.2
  89.1 1.2 copy_dynamic-update-slice_fusion.1
  90.3 1.2 copy_dynamic-update-slice_fusion
  91.5 4.5 %fusion.51 = (f32[4,2,4,16]{3,2,1,0:T(4,128)S(1)}, f32[4,2,4,16,8,32]{5,3,4,2,1,0:T(8,128)S(1)}) fusion(f32[2,4,16,32,4,8]{3,5,4,2,1,0:T(8,128)S(1)} %copy-done.1, bf16[4,8,2,4,32,2,64]{6,4,1,3,5,0,2:T(8,128)(2,1)} %copy_dynamic-update-slice_fusion, pred[4,16,32]{2,1,0:T(8,128)(4,1)S(1)} %copy-done.8, f32[64]{0:T(128)S(1)} %convert_element_type.95, ...), kind=kOutput, calls=%fused_computation.97 | convolution fusion | flops 17399296 | bytes 3283200 | tf_op jit(solution)/shard_map/rbqhd,rjbkhd->rhbqjk/dot_general | solution.py:156
  96.1 0.9 copy.124
  96.9 0.6 reshape.302
  97.6 1.0 fusion.47
  98.7 0.4 fusion.52
  99.1 0.5 fusion.18
  99.6 0.4 divide_convert_fusion
  100.0 0.4 reshape.279
  100.4 2.5 %fusion.12 = f32[4,4,16,2,64]{4,2,3,1,0:T(8,128)S(1)} fusion(bf16[4,2,4,16,8,32]{5,4,3,2,0,1:T(8,128)(2,1)S(1)} %reshape.279, bf16[4,8,2,4,32,2,64]{6,4,1,3,5,0,2:T(8,128)(2,1)} %copy_dynamic-update-slice_fusion), kind=kOutput, calls=%fused_computation.23 | convolution fusion | flops 16777216 | bytes 2490368 | tf_op jit(solution)/shard_map/rhbqjk,rjbkhd->rbqhd/dot_general | solution.py:173
  103.0 0.3 fusion.16
  103.6 0.8 broadcast_in_dim.30
  104.5 5.6 %all-to-all-start.2 = ((bf16[8,256,128]{1,2,0:T(8,128)(2,1)}), bf16[8,256,128]{1,2,0:T(8,128)(2,1)S(1)}, u32[]{:S(2)}, u32[]{:S(2)}) async-start(bf16[8,256,128]{1,2,0:T(8,128)(2,1)} %broadcast_in_dim.30), calls=%async_computation.2 | async-start | bytes 1048576 | tf_op jit(solution)/shard_map/all_to_all | solution.py:30
  110.2 9.3 %all-to-all-done.2 = bf16[8,256,128]{1,2,0:T(8,128)(2,1)S(1)} async-done(((bf16[8,256,128]{1,2,0:T(8,128)(2,1)}), bf16[8,256,128]{1,2,0:T(8,128)(2,1)S(1)}, u32[]{:S(2)}, u32[]{:S(2)}) %all-to-all-start.2) | async-done | bytes 524320 | tf_op jit(solution)/shard_map/all_to_all | solution.py:30
  119.5 1.9 %fusion.17 = bf16[256,256]{1,0:T(8,128)(2,1)} fusion(bf16[256,1024]{0,1:T(8,128)(2,1)S(1)} %bitcast.121, bf16[1024,256]{1,0:T(8,128)(2,1)S(1)} %copy-done.10, f32[256]{0:T(256)S(1)} %dynamic_slice.7, bf16[256,2048]{1,0:T(8,128)(2,1)} %param.17, s32[]{:T(128)S(6)} %select_n.28), kind=kOutput, calls=%fused_computation.27 | convolution fusion | flops 134479872 | bytes 1311748 | tf_op jit(solution)/shard_map/dot_general | solution.py:180
  (73 shorter events, 2.4 us)
Async XLA Ops:
  0.0 62.5 %copy-start = (bf16[2048,128]{1,0:T(8,128)(2,1)S(1)}, bf16[2048,128]{1,0:T(8,128)(2,1)}, u32[]{:S(2)}) copy-start(bf16[2048,128]{1,0:T(8,128)(2,1)} %param.26) | copy-start | bytes 1572868
  0.0 53.9 %copy-start.5 = (f32[4,16,32,31,1]{3,2,1,0,4:T(8,128)S(1)}, f32[4,16,32,31,1]{3,2,1,0,4:T(8,128)}, u32[]{:S(2)}) copy-start(f32[4,16,32,31,1]{3,2,1,0,4:T(8,128)} %constant.87) | copy-start | bytes 761860
  38.6 23.3 %all-to-all-start = ((f32[8,5,256]{2,1,0:T(8,128)}), f32[8,5,256]{2,1,0:T(8,128)S(1)}, u32[]{:S(2)}, u32[]{:S(2)}) async-start(f32[8,5,256]{2,1,0:T(8,128)} %broadcast_in_dim.24), calls=%async_computation | async-start | bytes 131072 | tf_op jit(solution)/shard_map/all_to_all | solution.py:30
  59.4 2.4 %copy-start.9 = (bf16[2048]{0:T(1024)(128)(2,1)S(1)}, bf16[2048]{0:T(1024)(128)(2,1)}, u32[]{:S(2)}) copy-start(bf16[2048]{0:T(1024)(128)(2,1)} %param.24) | copy-start | bytes 12292
  59.4 2.4 %copy-start.11 = (bf16[64]{0:T(256)(128)(2,1)S(1)}, bf16[64]{0:T(256)(128)(2,1)}, u32[]{:S(2)}) copy-start(bf16[64]{0:T(256)(128)(2,1)} %param.29) | copy-start | bytes 388
  59.5 2.5 %copy-start.12 = (bf16[64]{0:T(256)(128)(2,1)S(1)}, bf16[64]{0:T(256)(128)(2,1)}, u32[]{:S(2)}) copy-start(bf16[64]{0:T(256)(128)(2,1)} %param.28) | copy-start | bytes 388
  59.5 2.5 %copy-start.2 = (bf16[256,2048]{1,0:T(8,128)(2,1)S(1)}, bf16[256,2048]{1,0:T(8,128)(2,1)}, u32[]{:S(2)}) copy-start(bf16[256,2048]{1,0:T(8,128)(2,1)} %param.17) | copy-start | bytes 3145732
  62.5 1.3 %copy-start.4 = (bf16[2048,128]{1,0:T(8,128)(2,1)S(1)}, bf16[2048,128]{1,0:T(8,128)(2,1)}, u32[]{:S(2)}) copy-start(bf16[2048,128]{1,0:T(8,128)(2,1)} %param.27) | copy-start | bytes 1572868
  62.9 4.4 %copy-start.7 = (bf16[8,2048]{1,0:T(8,128)(2,1)S(1)}, bf16[8,2048]{1,0:T(8,128)(2,1)}, u32[]{:S(2)}) copy-start(bf16[8,2048]{1,0:T(8,128)(2,1)} %param.18) | copy-start | bytes 98308
  63.2 4.6 %copy-start.6 = (bf16[2048,128]{1,0:T(8,128)(2,1)S(1)}, bf16[2048,128]{1,0:T(8,128)(2,1)}, u32[]{:S(2)}) copy-start(bf16[2048,128]{1,0:T(8,128)(2,1)} %param.25) | copy-start | bytes 1572868
  64.2 15.4 %collective-permute-start = (bf16[4,2,64,128]{3,2,0,1:T(8,128)(2,1)S(1)}, bf16[4,2,64,128]{3,2,0,1:T(8,128)(2,1)S(1)}, u32[]{:S(2)}, u32[]{:S(2)}) collective-permute-start(bf16[4,2,64,128]{3,2,0,1:T(8,128)(2,1)S(1)} %pad_maximum_fusion.1), channel_id=1, source_target_pairs={{0,8},{8,16},{16,24},{24,32},{32,40},{40,48},{48,56},{56,64},{64,7... | collective-permute-start | bytes 393224 | tf_op jit(solution)/shard_map/ppermute | solution.py:49
  66.0 13.6 %collective-permute-start.1 = (bf16[4,2,64,128]{3,2,0,1:T(8,128)(2,1)S(1)}, bf16[4,2,64,128]{3,2,0,1:T(8,128)(2,1)S(1)}, u32[]{:S(2)}, u32[]{:S(2)}) collective-permute-start(bf16[4,2,64,128]{3,2,0,1:T(8,128)(2,1)S(1)} %pad_maximum_fusion.1), channel_id=1, source_target_pairs={{8,0},{16,8},{24,16},{32,24},{40,32},{48,40},{56,48},{64,56},{72,6... | collective-permute-start | bytes 393224 | tf_op jit(solution)/shard_map/ppermute | solution.py:52
  69.8 27.7 %all-to-all-start.1 = ((bf16[64,8,256]{2,1,0:T(8,128)(2,1)}), bf16[64,8,256]{2,1,0:T(8,128)(2,1)}, u32[]{:S(2)}, u32[]{:S(2)}) async-start(bf16[64,8,256]{2,1,0:T(8,128)(2,1)} %broadcast_in_dim.29), calls=%async_computation.1 | async-start | bytes 524288 | tf_op jit(solution)/shard_map/all_to_all | solution.py:30
  87.9 2.4 %copy-start.3 = (bf16[4,8,2,1,32,2,64]{6,5,4,2,1,0,3:T(2,128)(2,1)S(1)}, bf16[4,8,2,1,32,2,64]{6,5,4,2,1,0,3:T(2,128)(2,1)}, u32[]{:S(2)}) copy-start(bf16[4,8,2,1,32,2,64]{6,5,4,2,1,0,3:T(2,128)(2,1)} %stack.34) | copy-start | bytes 1572868
  89.1 2.4 %copy-start.1 = (f32[2,4,16,32,4,8]{3,5,4,2,1,0:T(8,128)S(1)}, f32[2,4,16,32,4,8]{3,5,4,2,1,0:T(8,128)}, u32[]{:S(2)}) copy-start(f32[2,4,16,32,4,8]{3,5,4,2,1,0:T(8,128)} %fusion.32) | copy-start | bytes 1572868
  89.1 2.4 %copy-start.8 = (pred[4,16,32]{2,1,0:T(8,128)(4,1)S(1)}, pred[4,16,32]{2,1,0:T(8,128)(4,1)}, u32[]{:S(2)}) copy-start(pred[4,16,32]{2,1,0:T(8,128)(4,1)} %constant.79.clone) | copy-start | bytes 6148
  102.9 16.6 %copy-start.10 = (bf16[1024,256]{1,0:T(8,128)(2,1)S(1)}, bf16[1024,256]{1,0:T(8,128)(2,1)}, u32[]{:S(2)}) copy-start(bf16[1024,256]{1,0:T(8,128)(2,1)} %param.31) | copy-start | bytes 1572868
  104.5 15.0 %all-to-all-start.2 = ((bf16[8,256,128]{1,2,0:T(8,128)(2,1)}), bf16[8,256,128]{1,2,0:T(8,128)(2,1)S(1)}, u32[]{:S(2)}, u32[]{:S(2)}) async-start(bf16[8,256,128]{1,2,0:T(8,128)(2,1)} %broadcast_in_dim.30), calls=%async_computation.2 | async-start | bytes 1048576 | tf_op jit(solution)/shard_map/all_to_all | solution.py:30
where the time goes:
time: 122 us; the launch traced here: 121 us
  blocking collectives  34.6 us (28%)
  starting transfers between devices  31 us (25%)
  matrix products  21.9 us (18%)
  local copies, waits for them, and re-layouts  18.9 us (15%)
  waiting for transfers between devices  9.29 us (8%)
  other arithmetic  5.2 us (4%)
    psum x2, blocking collectives, one_axis_at_a_time(): x = lax.psum(x, axis)  34.6 us
    all_to_all x3, starting transfers between devices, sent_to_all(): return lax.all_to_all(copies, axis, split_axis=0, concat_axis=0, tiled=True)  27.9 us
    all_to_all x3, waiting for transfers between devices, sent_to_all(): return lax.all_to_all(copies, axis, split_axis=0, concat_axis=0, tiled=True)  9.28 us
    another operation x5, local copies, waits for them, and re-layouts, body(): jnp.stack([band[:, :, :, begin:begin + span] for begin in starts], axis=3)  5.84 us
    dot_general x1, matrix products, body(): jnp.einsum('hxc,bqkc->hxbqk', offset_bias, jnp.asarray(col_onehot), preci...  5.56 us
    dot_general x1, matrix products, body(): jnp.einsum('rbqhd,rjbkhd->rhbqjk', grid_q, key_blocks, preferred_element_...  4.53 us
    unnamed x29, local copies, waits for them, and re-layouts  3.67 us
    dot_general x1, matrix products, body(): jnp.einsum('rhbqjk,rjbkhd->rbqhd', local_w, value_blocks, preferred_eleme...  2.47 us
  transfers between devices with their start and end apart: 5, of which 1 were waited for; matrix products, arithmetic and copies ran while one was open for 26% of the time, Pallas kernels for 0%

commit v1 on v0

--- a/solution.py
+++ b/solution.py
@@ -15,7 +15,7 @@
 
 def one_axis_at_a_time(x, axes):
     for axis in axes:
-        x = lax.psum(x, axis)
+        x = jnp.sum(lax.all_gather(x, axis), axis=0)
     return x
 
 

time: 122 us -> 140 us (1.15)
  blocking collectives: 34.6 us -> 45.8 us
  starting transfers between devices: 31 us -> 38.1 us
    all_gather x0 -> x2, blocking collectives: none -> 45.8 us  [one_axis_at_a_time(): x = jnp.sum(lax.all_gather(x, axis), axis=0)]
    psum x2 -> x0, blocking collectives: 34.6 us -> none  [one_axis_at_a_time(): x = lax.psum(x, axis)]
    all_to_all x3, starting transfers between devices: 27.9 us -> 34.5 us  [sent_to_all(): return lax.all_to_all(copies, axis, split_axis=0, concat_axis=0, tiled=True)]
  transfers between devices with their start and end apart: 5 -> 5, of which waited for: 1 -> 1; matrix products, arithmetic and copies ran while one was open for 26% -> 22% of each run, Pallas kernels for 0% -> 0%
where the time goes in v1:
time: 140 us
  blocking collectives  45.8 us (33%)
  starting transfers between devices  38.1 us (27%)
  matrix products  21.9 us (16%)
  local copies, waits for them, and re-layouts  18.9 us (13%)
  waiting for transfers between devices  9.29 us (7%)
  other arithmetic  5.23 us (4%)
    all_gather x2, blocking collectives, one_axis_at_a_time(): x = jnp.sum(lax.all_gather(x, axis), axis=0)  45.8 us
    all_to_all x3, starting transfers between devices, sent_to_all(): return lax.all_to_all(copies, axis, split_axis=0, concat_axis=0, tiled=True)  34.5 us
    all_to_all x3, waiting for transfers between devices, sent_to_all(): return lax.all_to_all(copies, axis, split_axis=0, concat_axis=0, tiled=True)  9.28 us
    another operation x5, local copies, waits for them, and re-layouts, body(): jnp.stack([band[:, :, :, begin:begin + span] for begin in starts], axis=3)  5.84 us
    dot_general x1, matrix products, body(): jnp.einsum('hxc,bqkc->hxbqk', offset_bias, jnp.asarray(col_onehot), preci...  5.56 us
    dot_general x1, matrix products, body(): jnp.einsum('rbqhd,rjbkhd->rhbqjk', grid_q, key_blocks, preferred_element_...  4.53 us
    unnamed x29, local copies, waits for them, and re-layouts  3.67 us
  transfers between devices with their start and end apart: 5, of which 1 were waited for; matrix products, arithmetic and copies ran while one was open for 22% of the time, Pallas kernels for 0%

profile of v1, /device:TPU:1, one launch (start us, length us, event | category | flops | bytes accessed | tf_op | source)
XLA Modules:
  0.0 139.6 jit_solution(13964885250409873426)
XLA Ops:
  0.0 0.8 convert_bitcast_fusion
  0.8 0.8 fusion.42
  1.7 0.8 fusion.41
  2.5 0.9 fusion.38
  3.4 25.7 %all-gather.2 = f32[8,5,256]{2,1,0:T(8,128)S(1)} all-gather(f32[1,5,256]{2,1,0:T(8,128)S(1)} %maximum_bitcast_fusion), channel_id=2, replica_groups=mesh['sp_0'=8,'sp_1'=8,'tp'=8] {'sp_0'}, dimensions={0}, use_global_device_ids=true | all-gather | bytes 46080 | tf_op jit(solution)/shard_map/all_gather | solution.py:18
  29.1 20.1 %all-gather.3 = f32[8,5,256]{2,1,0:T(8,128)S(1)} all-gather(f32[1,5,256]{2,1,0:T(8,128)S(1)} %bitcast.134), channel_id=3, replica_groups=mesh['sp_0'=8,'sp_1'=8,'tp'=8] {'sp_1'}, dimensions={0}, use_global_device_ids=true | all-gather | bytes 46080 | tf_op jit(solution)/shard_map/all_gather | solution.py:18
  49.2 0.6 broadcast_in_dim.24
  49.8 17.1 %all-to-all-start = ((f32[8,5,256]{2,1,0:T(8,128)}), f32[8,5,256]{2,1,0:T(8,128)S(1)}, u32[]{:S(2)}, u32[]{:S(2)}) async-start(f32[8,5,256]{2,1,0:T(8,128)} %broadcast_in_dim.24), calls=%async_computation | async-start | bytes 131072 | tf_op jit(solution)/shard_map/all_to_all | solution.py:30
  67.1 1.5 %fusion = f32[256]{0:T(256)S(1)} fusion(bf16[256,2048]{1,0:T(8,128)(2,1)} %param.17), kind=kLoop, calls=%fused_computation.3 | loop fusion | flops 1572608 | bytes 1049600 | tf_op jit(solution)/shard_map/reduce_sum | solution.py:59
  68.7 0.9 fusion.25
  69.7 5.6 %convolution_bitcast_fusion = f32[2,15,4,16,32,1]{4,1,5,3,2,0:T(8,128)S(1)} fusion(f32[4,16,32,31,1]{3,2,1,0,4:T(8,128)S(1)} %copy-done.5, f32[2,15,31,1,1]{2,0,1,4,3:T(2,128)} %bitcast.135), kind=kOutput, calls=%fused_computation.20 | convolution fusion | flops 22855680 | bytes 503432 | tf_op jit(solution)/shard_map/hxc,bqkc->hxbqk/dot_general | solution.py:149
  75.3 2.3 %fusion.32 = f32[2,4,16,32,4,8]{3,5,4,2,1,0:T(8,128)} fusion(f32[2,15,4,16,32,1]{4,1,5,3,2,0:T(8,128)S(1)} %convolution_bitcast_fusion, s32[4,8]{1,0:T(4,128)S(1)} %subtract_add_fusion), kind=kOutput, calls=%fused_computation.59 | convolution fusion | flops 23593440 | bytes 770176 | tf_op jit(solution)/shard_map/rjx,hxbqk->rhbqjk/dot_general | solution.py:152
  77.8 0.5 fusion.4
  78.3 0.4 fusion.49
  79.1 0.3 mul.200
  79.6 0.4 convolution_convert_fusion
  80.1 2.3 %collective-permute-start = (bf16[4,2,64,128]{3,2,0,1:T(8,128)(2,1)S(1)}, bf16[4,2,64,128]{3,2,0,1:T(8,128)(2,1)S(1)}, u32[]{:S(2)}, u32[]{:S(2)}) collective-permute-start(bf16[4,2,64,128]{3,2,0,1:T(8,128)(2,1)S(1)} %pad_maximum_fusion.1), channel_id=1, source_target_pairs={{0,8},{8,16},{16,24},{24,32},{32,40},{40,48},{48,56},{56,64},{64,7... | collective-permute-start | bytes 393224 | tf_op jit(solution)/shard_map/ppermute | solution.py:49
  82.4 1.3 collective-permute-start.1
  83.7 0.2 fusion.50
  83.9 0.2 convolution_convert_fusion.1
  84.2 0.5 bitcast_reduce_fusion
  85.1 0.2 reshape.275
  85.5 0.7 broadcast_in_dim.29
  86.2 11.7 %all-to-all-start.1 = ((bf16[64,8,256]{2,1,0:T(8,128)(2,1)}), bf16[64,8,256]{2,1,0:T(8,128)(2,1)}, u32[]{:S(2)}, u32[]{:S(2)}) async-start(bf16[64,8,256]{2,1,0:T(8,128)(2,1)} %broadcast_in_dim.29), calls=%async_computation.1 | async-start | bytes 524288 | tf_op jit(solution)/shard_map/all_to_all | solution.py:30
  98.0 0.7 gather_fusion
  98.9 1.4 %fusion.46 = (bf16[4,8,2,32,128]{4,3,2,1,0:T(8,128)(2,1)S(1)}, bf16[4,8,2,32,128]{4,3,2,1,0:T(8,128)(2,1)}, bf16[4,8,2,32,128]{4,3,2,1,0:T(8,128)(2,1)S(1)}, bf16[4,8,2,32,128]{4,3,2,1,0:T(8,128)(2,1)S(1)}) fusion(bf16[4,8,2,64,128]{4,3,2,1,0:T(8,128)(2,1)S(1)} %broadcast_select_fusion), kind=kLoop, calls=%fused_computation.92 | loop fusion | bytes 4194304 | tf_op jit(solution)/shard_map/slice | solution.py:135
  100.3 0.4 stack.31
  100.7 1.2 copy_dynamic-update-slice_fusion.3
  101.9 0.4 stack.32
  102.3 2.5 %stack.33 = bf16[4,8,2,1,32,2,64]{6,5,4,2,1,0,3:T(2,128)(2,1)S(1)} reshape(bf16[4,8,2,32,128]{4,3,2,1,0:T(8,128)(2,1)} %get-tuple-element.6) | data formatting | bytes 1048576 | tf_op jit(solution)/shard_map/stack | solution.py:135
  104.8 1.4 %stack.34 = bf16[4,8,2,1,32,2,64]{6,5,4,2,1,0,3:T(2,128)(2,1)} reshape(bf16[4,8,2,32,128]{4,3,2,1,0:T(8,128)(2,1)S(1)} %get-tuple-element.5) | data formatting | bytes 1048576 | tf_op jit(solution)/shard_map/stack | solution.py:135
  106.2 1.2 copy_dynamic-update-slice_fusion.2
  107.4 1.2 copy_dynamic-update-slice_fusion.1
  108.6 1.2 copy_dynamic-update-slice_fusion
  109.8 4.5 %fusion.51 = (f32[4,2,4,16]{3,2,1,0:T(4,128)S(1)}, f32[4,2,4,16,8,32]{5,3,4,2,1,0:T(8,128)S(1)}) fusion(f32[2,4,16,32,4,8]{3,5,4,2,1,0:T(8,128)S(1)} %copy-done.1, bf16[4,8,2,4,32,2,64]{6,4,1,3,5,0,2:T(8,128)(2,1)} %copy_dynamic-update-slice_fusion, pred[4,16,32]{2,1,0:T(8,128)(4,1)S(1)} %copy-done.8, f32[64]{0:T(128)S(1)} %convert_element_type.95, ...), kind=kOutput, calls=%fused_computation.97 | convolution fusion | flops 17399296 | bytes 3283200 | tf_op jit(solution)/shard_map/rbqhd,rjbkhd->rhbqjk/dot_general | solution.py:156
  114.3 0.9 copy.124
  115.2 0.6 reshape.310
  115.8 1.0 fusion.47
  116.9 0.4 fusion.52
  117.4 0.5 fusion.18
  117.8 0.4 divide_convert_fusion
  118.2 0.4 reshape.279
  118.7 2.5 %fusion.12 = f32[4,4,16,2,64]{4,2,3,1,0:T(8,128)S(1)} fusion(bf16[4,2,4,16,8,32]{5,4,3,2,0,1:T(8,128)(2,1)S(1)} %reshape.279, bf16[4,8,2,4,32,2,64]{6,4,1,3,5,0,2:T(8,128)(2,1)} %copy_dynamic-update-slice_fusion), kind=kOutput, calls=%fused_computation.23 | convolution fusion | flops 16777216 | bytes 2490368 | tf_op jit(solution)/shard_map/rhbqjk,rjbkhd->rbqhd/dot_general | solution.py:173
  121.3 0.3 fusion.16
  121.9 0.8 broadcast_in_dim.30
  122.7 5.7 %all-to-all-start.2 = ((bf16[8,256,128]{1,2,0:T(8,128)(2,1)}), bf16[8,256,128]{1,2,0:T(8,128)(2,1)S(1)}, u32[]{:S(2)}, u32[]{:S(2)}) async-start(bf16[8,256,128]{1,2,0:T(8,128)(2,1)} %broadcast_in_dim.30), calls=%async_computation.2 | async-start | bytes 1048576 | tf_op jit(solution)/shard_map/all_to_all | solution.py:30
  128.4 9.3 %all-to-all-done.2 = bf16[8,256,128]{1,2,0:T(8,128)(2,1)S(1)} async-done(((bf16[8,256,128]{1,2,0:T(8,128)(2,1)}), bf16[8,256,128]{1,2,0:T(8,128)(2,1)S(1)}, u32[]{:S(2)}, u32[]{:S(2)}) %all-to-all-start.2) | async-done | bytes 524320 | tf_op jit(solution)/shard_map/all_to_all | solution.py:30
  137.7 1.9 %fusion.17 = bf16[256,256]{1,0:T(8,128)(2,1)} fusion(bf16[256,1024]{0,1:T(8,128)(2,1)S(1)} %bitcast.124, bf16[1024,256]{1,0:T(8,128)(2,1)S(1)} %copy-done.10, f32[256]{0:T(256)S(1)} %dynamic_slice.7, bf16[256,2048]{1,0:T(8,128)(2,1)} %param.17, s32[]{:T(128)S(6)} %select_n.28), kind=kOutput, calls=%fused_computation.27 | convolution fusion | flops 134479872 | bytes 1311748 | tf_op jit(solution)/shard_map/dot_general | solution.py:180
  (75 shorter events, 2.5 us)
Async XLA Ops:
  0.0 78.3 %copy-start = (bf16[2048,128]{1,0:T(8,128)(2,1)S(1)}, bf16[2048,128]{1,0:T(8,128)(2,1)}, u32[]{:S(2)}) copy-start(bf16[2048,128]{1,0:T(8,128)(2,1)} %param.26) | copy-start | bytes 1572868
  0.0 69.7 %copy-start.5 = (f32[4,16,32,31,1]{3,2,1,0,4:T(8,128)S(1)}, f32[4,16,32,31,1]{3,2,1,0,4:T(8,128)}, u32[]{:S(2)}) copy-start(f32[4,16,32,31,1]{3,2,1,0,4:T(8,128)} %constant.87) | copy-start | bytes 761860
  49.8 27.9 %all-to-all-start = ((f32[8,5,256]{2,1,0:T(8,128)}), f32[8,5,256]{2,1,0:T(8,128)S(1)}, u32[]{:S(2)}, u32[]{:S(2)}) async-start(f32[8,5,256]{2,1,0:T(8,128)} %broadcast_in_dim.24), calls=%async_computation | async-start | bytes 131072 | tf_op jit(solution)/shard_map/all_to_all | solution.py:30
  75.3 2.4 %copy-start.9 = (bf16[2048]{0:T(1024)(128)(2,1)S(1)}, bf16[2048]{0:T(1024)(128)(2,1)}, u32[]{:S(2)}) copy-start(bf16[2048]{0:T(1024)(128)(2,1)} %param.24) | copy-start | bytes 12292
  75.3 2.4 %copy-start.11 = (bf16[64]{0:T(256)(128)(2,1)S(1)}, bf16[64]{0:T(256)(128)(2,1)}, u32[]{:S(2)}) copy-start(bf16[64]{0:T(256)(128)(2,1)} %param.29) | copy-start | bytes 388
  75.3 2.5 %copy-start.12 = (bf16[64]{0:T(256)(128)(2,1)S(1)}, bf16[64]{0:T(256)(128)(2,1)}, u32[]{:S(2)}) copy-start(bf16[64]{0:T(256)(128)(2,1)} %param.28) | copy-start | bytes 388
  75.3 2.5 %copy-start.2 = (bf16[256,2048]{1,0:T(8,128)(2,1)S(1)}, bf16[256,2048]{1,0:T(8,128)(2,1)}, u32[]{:S(2)}) copy-start(bf16[256,2048]{1,0:T(8,128)(2,1)} %param.17) | copy-start | bytes 3145732
  78.3 1.3 copy-start.4
  78.8 4.9 %copy-start.7 = (bf16[8,2048]{1,0:T(8,128)(2,1)S(1)}, bf16[8,2048]{1,0:T(8,128)(2,1)}, u32[]{:S(2)}) copy-start(bf16[8,2048]{1,0:T(8,128)(2,1)} %param.18) | copy-start | bytes 98308
  79.1 5.1 %copy-start.6 = (bf16[2048,128]{1,0:T(8,128)(2,1)S(1)}, bf16[2048,128]{1,0:T(8,128)(2,1)}, u32[]{:S(2)}) copy-start(bf16[2048,128]{1,0:T(8,128)(2,1)} %param.25) | copy-start | bytes 1572868
  80.1 17.8 %collective-permute-start = (bf16[4,2,64,128]{3,2,0,1:T(8,128)(2,1)S(1)}, bf16[4,2,64,128]{3,2,0,1:T(8,128)(2,1)S(1)}, u32[]{:S(2)}, u32[]{:S(2)}) collective-permute-start(bf16[4,2,64,128]{3,2,0,1:T(8,128)(2,1)S(1)} %pad_maximum_fusion.1), channel_id=1, source_target_pairs={{0,8},{8,16},{16,24},{24,32},{32,40},{40,48},{48,56},{56,64},{64,7... | collective-permute-start | bytes 393224 | tf_op jit(solution)/shard_map/ppermute | solution.py:49
  82.4 15.5 %collective-permute-start.1 = (bf16[4,2,64,128]{3,2,0,1:T(8,128)(2,1)S(1)}, bf16[4,2,64,128]{3,2,0,1:T(8,128)(2,1)S(1)}, u32[]{:S(2)}, u32[]{:S(2)}) collective-permute-start(bf16[4,2,64,128]{3,2,0,1:T(8,128)(2,1)S(1)} %pad_maximum_fusion.1), channel_id=1, source_target_pairs={{8,0},{16,8},{24,16},{32,24},{40,32},{48,40},{56,48},{64,56},{72,6... | collective-permute-start | bytes 393224 | tf_op jit(solution)/shard_map/ppermute | solution.py:52
  86.2 29.6 %all-to-all-start.1 = ((bf16[64,8,256]{2,1,0:T(8,128)(2,1)}), bf16[64,8,256]{2,1,0:T(8,128)(2,1)}, u32[]{:S(2)}, u32[]{:S(2)}) async-start(bf16[64,8,256]{2,1,0:T(8,128)(2,1)} %broadcast_in_dim.29), calls=%async_computation.1 | async-start | bytes 524288 | tf_op jit(solution)/shard_map/all_to_all | solution.py:30
  106.2 2.4 %copy-start.3 = (bf16[4,8,2,1,32,2,64]{6,5,4,2,1,0,3:T(2,128)(2,1)S(1)}, bf16[4,8,2,1,32,2,64]{6,5,4,2,1,0,3:T(2,128)(2,1)}, u32[]{:S(2)}) copy-start(bf16[4,8,2,1,32,2,64]{6,5,4,2,1,0,3:T(2,128)(2,1)} %stack.34) | copy-start | bytes 1572868
  107.4 2.4 %copy-start.1 = (f32[2,4,16,32,4,8]{3,5,4,2,1,0:T(8,128)S(1)}, f32[2,4,16,32,4,8]{3,5,4,2,1,0:T(8,128)}, u32[]{:S(2)}) copy-start(f32[2,4,16,32,4,8]{3,5,4,2,1,0:T(8,128)} %fusion.32) | copy-start | bytes 1572868
  107.4 2.4 %copy-start.8 = (pred[4,16,32]{2,1,0:T(8,128)(4,1)S(1)}, pred[4,16,32]{2,1,0:T(8,128)(4,1)}, u32[]{:S(2)}) copy-start(pred[4,16,32]{2,1,0:T(8,128)(4,1)} %constant.79.clone) | copy-start | bytes 6148
  121.1 16.6 %copy-start.10 = (bf16[1024,256]{1,0:T(8,128)(2,1)S(1)}, bf16[1024,256]{1,0:T(8,128)(2,1)}, u32[]{:S(2)}) copy-start(bf16[1024,256]{1,0:T(8,128)(2,1)} %param.31) | copy-start | bytes 1572868
  122.7 15.0 %all-to-all-start.2 = ((bf16[8,256,128]{1,2,0:T(8,128)(2,1)}), bf16[8,256,128]{1,2,0:T(8,128)(2,1)S(1)}, u32[]{:S(2)}, u32[]{:S(2)}) async-start(bf16[8,256,128]{1,2,0:T(8,128)(2,1)} %broadcast_in_dim.30), calls=%async_computation.2 | async-start | bytes 1048576 | tf_op jit(solution)/shard_map/all_to_all | solution.py:30
